TPU v7x, 32 devices: a whole 2x2x4 slice. The times are simulated.
32 devices in a mesh: grp: 2 (over y), ep: 4 (over z), tp: 4 (over x, core).
Axes of the slice: x: 2, y: 2, z: 4, core: 2. Of those that a mesh axis runs over, the one named last changes fastest.
Arguments:
- scan_branch_source: bfloat16 [1024, 1344], P(('grp', 'ep'), 'tp'), parts along dimension 0, may hold values from -8 to 8
- valve_branch_source: bfloat16 [1024, 1344], P(('grp', 'ep'), 'tp'), parts along dimension 0, may hold values from -6 to 6
- stencil_factors: bfloat16 [4, 1344], P(None, 'tp'), may hold values from -3 to 3
- carry_valve_matrix: bfloat16 [8, 168, 168], P('tp'), may hold values from -0.5 to 0.5
- entry_valve_matrix: bfloat16 [8, 168, 168], P('tp'), may hold values from -0.5 to 0.5
- lane_fade_param: float32 [1344], P('tp'), may hold values from 0 to 16
- jump_log_fade: float32 [1024], P(('grp', 'ep')), parts along dimension 0, may hold values from -0.6 to 0, as said below
- specialist_entries: bfloat16 [2048, 2048], P(('grp', 'ep')), parts along dimension 0, may hold values from -6 to 6
- specialist_rms_scale: float32 [2048], replicated, may hold values from 0.1 to 1.9
- assigned_specialists: int32 [2048, 2], P(('grp', 'ep')), parts along dimension 0, may hold values from 0 to 3, all different within a row; in each aligned block of 256 rows (0 to 255, 256 to 511, ...) at most 192 rows name the same one
- picked_route_scores: float32 [2048, 2], P(('grp', 'ep')), parts along dimension 0, may hold values from -6 to 6
- expand_matrix: bfloat16 [4, 2048, 3584], P('ep', None, 'tp'), may hold values from -0.125 to 0.125
- contract_matrix: bfloat16 [4, 3584, 2048], P('ep', None, 'tp'), may hold values from -0.09375 to 0.09375
Outputs:
- valved_scan_target: bfloat16 [1024, 1344], P(('grp', 'ep'), 'tp'), parts along dimension 0
- moe_out: bfloat16 [2048, 2048], P(('grp', 'ep'), 'tp'), parts along dimension 0
There are 2 independent parts, one for each index of `grp`. A program takes and returns all parts, laid end to end along the dimension named above; an argument that names none is the same for every part. Nothing has to cross between parts.
Inputs may be any that keep to these rules, and one draw needn't show every extreme that they name: `assigned_specialists`: each row names 2 different experts. Among the tokens of one index of ep (aligned blocks of 256 rows) no expert is named more than 192 times, and in some block some expert is named exactly 192 times. `jump_log_fade`: zero at all but a few positions.
All inputs are finite; a program needn't handle non-finite values.
Results may differ from a plain program's by a relative error of at most 0.0065.
Values may be sent and summed in bfloat16 or wider, within the bound.
A program may use at most 128 MiB of HBM per device.

v0:
```python
import functools

import jax
import jax.numpy as jnp
from jax import lax
from jax.experimental import pallas as pl
from jax.experimental.pallas import tpu as pltpu
from jax.sharding import PartitionSpec as P

CONV = 4


def passed_along(block, axis, distance):
    devices = range(lax.axis_size(axis))
    route = [(i - distance, i) for i in devices if i - distance in devices]
    return lax.ppermute(block, axis, route)


def carried_in(part, axis, combine, identity):
    place = lax.axis_index(axis)
    gathered = jax.tree.map(lambda a: lax.all_gather(a, axis), part)
    state = jax.tree.map(lambda a, e: jnp.zeros_like(a) + jnp.asarray(e, a.dtype), part, identity)

    def one(step, state):
        return combine(
            state, jax.tree.map(lambda a: lax.dynamic_index_in_dim(a, step, 0, False), gathered)
        )

    return lax.fori_loop(0, place, one, state)


def chain_link(earlier, later):
    early_decay, early_state = earlier
    late_decay, late_state = later
    return (early_decay * late_decay, late_decay * early_state + late_state)


def slot_table(assigned_specialists, experts, capacity):
    flat_routes = assigned_specialists.reshape(-1)
    top_count = assigned_specialists.shape[1]
    matches = (flat_routes[:, None] == jnp.arange(experts, dtype=jnp.int32)[None, :]).astype(
        jnp.int32
    )
    before = jnp.cumsum(matches, axis=0) - matches
    slot_rank = jnp.sum(before * matches, axis=1)
    slot_index = flat_routes * capacity + slot_rank
    owner_row = jnp.arange(flat_routes.shape[0], dtype=jnp.int32) // top_count
    source = jnp.zeros((experts * capacity,), jnp.int32).at[slot_index].set(owner_row)
    filled = jnp.zeros((experts * capacity,), jnp.float32).at[slot_index].set(1.0)
    return (slot_index, source, filled)


def temporal_block_part(
    scan_branch_source,
    valve_branch_source,
    stencil_factors,
    carry_valve_matrix,
    entry_valve_matrix,
    lane_fade_param,
    jump_log_fade,
):
    length = scan_branch_source.shape[0]
    channels = scan_branch_source.shape[1]
    previous = passed_along(scan_branch_source[length - (CONV - 1) :], "ep", 1)
    padded = jnp.concatenate([previous, scan_branch_source], axis=0).astype(jnp.float32)
    tap_values = stencil_factors.astype(jnp.float32)
    conv_out = jnp.zeros((length, channels), jnp.float32)
    for offset in range(CONV):
        conv_out = conv_out + padded[offset : offset + length] * tap_values[offset]
    blocks_here = carry_valve_matrix.shape[0]
    conv_blocks = conv_out.astype(jnp.bfloat16).reshape(
        length, blocks_here, carry_valve_matrix.shape[1]
    )
    carry_valve = jax.nn.sigmoid(
        jnp.einsum(
            "tnc,ncd->tnd", conv_blocks, carry_valve_matrix, preferred_element_type=jnp.float32
        ).reshape(length, channels)
    )
    input_gate = jax.nn.sigmoid(
        jnp.einsum(
            "tnc,ncd->tnd", conv_blocks, entry_valve_matrix, preferred_element_type=jnp.float32
        ).reshape(length, channels)
    )
    fade_log_rate = (
        -8.0 * carry_valve * jax.nn.softplus(-lane_fade_param)[None, :] + jump_log_fade[:, None]
    )
    drive_term = jnp.sqrt(-jnp.expm1(2.0 * fade_log_rate)) * input_gate * conv_out
    cumulative, local_state = lax.associative_scan(
        chain_link, (jnp.exp(fade_log_rate), drive_term), axis=0
    )
    identity = (jnp.ones((channels,), jnp.float32), jnp.zeros((channels,), jnp.float32))
    entering = carried_in((cumulative[-1], local_state[-1]), "ep", chain_link, identity)
    hidden_state = local_state + cumulative * entering[1][None, :]
    return (hidden_state * jax.nn.gelu(valve_branch_source.astype(jnp.float32))).astype(
        jnp.bfloat16
    )


def expert_part(
    specialist_entries,
    specialist_rms_scale,
    assigned_specialists,
    picked_route_scores,
    expand_matrix,
    contract_matrix,
):
    ep_size = lax.axis_size("ep")
    tp_size = lax.axis_size("tp")
    exp_dev = expand_matrix.shape[0]
    experts = exp_dev * ep_size
    tokens = specialist_entries.shape[0]
    features = specialist_entries.shape[1]
    top_count = assigned_specialists.shape[1]
    capacity = tp_size * (
        (3 * tokens * top_count + 2 * experts * tp_size - 1) // (2 * experts * tp_size)
    )
    tok_rows = specialist_entries.astype(jnp.float32)
    row_mean = jnp.mean(tok_rows, axis=1, keepdims=True)
    centered = tok_rows - row_mean
    row_var = jnp.mean(centered * centered, axis=1, keepdims=True)
    normed = (centered * lax.rsqrt(row_var + 1e-05) * specialist_rms_scale[None, :]).astype(
        jnp.bfloat16
    )
    slot_index, source, filled = slot_table(assigned_specialists, experts, capacity)
    source_grid = source.reshape(experts, capacity)
    filled_grid = filled.reshape(experts, capacity)
    slice_size = capacity // tp_size
    first_slot = lax.axis_index("tp") * slice_size
    source_grid = lax.dynamic_slice_in_dim(source_grid, first_slot, slice_size, 1)
    filled_grid = lax.dynamic_slice_in_dim(filled_grid, first_slot, slice_size, 1)
    outgoing = normed[source_grid] * filled_grid[:, :, None].astype(jnp.bfloat16)
    outgoing = outgoing.reshape(ep_size, exp_dev, source_grid.shape[1], features)
    arrived = lax.all_to_all(outgoing, "ep", split_axis=0, concat_axis=0, tiled=True)
    arrived = lax.all_gather(arrived, "tp", axis=2, tiled=True)
    hidden = jax.nn.silu(
        jnp.einsum("secd,edf->secf", arrived, expand_matrix, preferred_element_type=jnp.float32)
    ).astype(jnp.bfloat16)
    column_count = contract_matrix.shape[2]
    expert_out = jnp.einsum(
        "secf,efd->secd",
        lax.all_gather(hidden, "tp", axis=3, tiled=True),
        contract_matrix,
        preferred_element_type=jnp.float32,
    ).astype(jnp.bfloat16)
    returned = lax.all_to_all(expert_out, "ep", split_axis=0, concat_axis=0, tiled=True)
    returned = returned.reshape(experts * capacity, column_count)
    picked = returned[slot_index].reshape(tokens, top_count, column_count).astype(jnp.float32)
    first_weight = jax.nn.sigmoid(picked_route_scores[:, 0] - picked_route_scores[:, 1])
    weights = jnp.stack([first_weight, 1.0 - first_weight], axis=1)
    return jnp.sum(weights[:, :, None] * picked, axis=1).astype(jnp.bfloat16)


MESH = pl.DeviceIdType.MESH
HALO = 16


def remote(src, dst, sems, index, **device):
    return pltpu.make_async_remote_copy(
        src_ref=src,
        dst_ref=dst,
        send_sem=sems.at[0, index],
        recv_sem=sems.at[1, index],
        device_id=device,
        device_id_type=MESH,
    )


def as_column(row):
    n = row.shape[1]
    same = lax.broadcasted_iota(jnp.int32, (n, n), 0) == lax.broadcasted_iota(jnp.int32, (n, n), 1)
    return jnp.sum(jnp.where(same, row, 0.0), axis=1, keepdims=True)


def one_minus_exp(x):
    near = jnp.maximum(x, -0.35)
    series = 1.0 + near * (1.0 / 8.0)
    for divisor in (7.0, 6.0, 5.0, 4.0, 3.0, 2.0):
        series = 1.0 + near * (1.0 / divisor) * series
    return jnp.where(x > -0.35, -near * series, 1.0 - jnp.exp(x))


def fused_kernel(
    n,
    capacity,
    scan_ref,
    valve_ref,
    taps_ref,
    carry_w_ref,
    entry_w_ref,
    lane_ref,
    jump_ref,
    tok_ref,
    gain_ref,
    route_ref,
    score_ref,
    up_hbm,
    down_hbm,
    scan_out,
    moe_out,
    up,
    down,
    normed,
    rank_rows,
    out_rows,
    toks,
    hid,
    res,
    back,
    halo,
    padded,
    conv_buf,
    decay_buf,
    state_buf,
    carry_out,
    carry_in,
    halo_out,
    acc,
    load_sems,
    zt,
    tx,
    tm,
    tf,
    hx,
    hm,
    hf,
    rz,
    halo_sems,
    carry_sems,
):
    e = lax.axis_index("ep")
    t = lax.axis_index("tp")
    mate = t + 1 - 2 * (t % 2)
    across = (t + 2) % 4
    far = (mate + 2) % 4
    tokens, features = tok_ref.shape
    part = features // 4
    width = up.shape[1]

    def f_cols(i):
        return pl.ds(pl.multiple_of(i * part, part), part)

    def h_cols(i):
        return pl.ds(pl.multiple_of(i * width, 128), width)

    barrier = pltpu.get_barrier_semaphore()
    for j in range(1, n):
        pl.semaphore_signal(barrier, inc=1, device_id={"ep": (e + j) % n}, device_id_type=MESH)
    for other in (mate, across):
        pl.semaphore_signal(barrier, inc=1, device_id={"tp": other}, device_id_type=MESH)
    load_up = pltpu.make_async_copy(up_hbm.at[0], up, load_sems.at[0])
    load_down = pltpu.make_async_copy(down_hbm.at[0], down, load_sems.at[1])
    load_up.start()
    load_down.start()
    channels, length = scan_ref.shape
    turned = scan_ref[...].astype(jnp.float32).T
    padded[HALO:, :] = turned
    halo_out[...] = turned[length - HALO :, :].astype(jnp.bfloat16)

    rows_step = 32

    def norm_rows(i, _):
        rows = pl.ds(pl.multiple_of(i * rows_step, rows_step), rows_step)
        x = tok_ref[rows, :].astype(jnp.float32)
        centered = x - jnp.sum(x, axis=1, keepdims=True) * (1.0 / features)
        var = jnp.sum(centered * centered, axis=1, keepdims=True) * (1.0 / features)
        normed[rows, :] = (centered * lax.rsqrt(var + 1e-05) * gain_ref[...]).astype(jnp.bfloat16)
        return 0

    lax.fori_loop(0, tokens // rows_step, norm_rows, 0)

    routes = route_ref[...].astype(jnp.float32)
    first, second = routes[0:1, :], routes[1:2, :]
    erow = lax.broadcasted_iota(jnp.int32, (rank_rows.shape[0], tokens), 0).astype(jnp.float32)
    hit = (erow == first) | (erow == second)
    ti = lax.broadcasted_iota(jnp.int32, (tokens, tokens), 0)
    tj = lax.broadcasted_iota(jnp.int32, (tokens, tokens), 1)
    rank = jnp.dot(
        hit.astype(jnp.float32).astype(jnp.bfloat16),
        (ti < tj).astype(jnp.float32).astype(jnp.bfloat16),
        preferred_element_type=jnp.float32,
    )
    rank_rows[...] = jnp.where(hit, rank, -1.0)

    def picker(expert):
        slots = lax.broadcasted_iota(jnp.int32, (capacity, tokens), 0).astype(jnp.float32)
        chosen = slots == rank_rows[pl.ds(expert, 1), :]
        return chosen.astype(jnp.float32).astype(jnp.bfloat16)

    pl.semaphore_wait(barrier, n + 1)

    send_halo = remote(halo_out, halo, halo_sems, 0, ep=(e + 1) % n)
    send_halo.start()

    def send_tokens(j):
        return remote(
            out_rows.at[j], toks.at[j, :, f_cols(t)], zt, j, ep=(e + n - j) % n
        )

    def dispatch(j, _):
        out_rows[j] = jnp.dot(
            picker((e + n - j) % n), normed[:, f_cols(t)], preferred_element_type=jnp.float32
        ).astype(jnp.bfloat16)
        send_tokens(j).start()
        return 0

    lax.fori_loop(1, n, dispatch, 0)

    mine = picker(e)
    for q in range(4):
        toks[0, :, q * part : (q + 1) * part] = jnp.dot(
            mine, normed[:, q * part : (q + 1) * part], preferred_element_type=jnp.float32
        ).astype(jnp.bfloat16)

    def hidden_block(j):
        for start in range(0, width, 256):
            size = min(256, width - start)
            value = jnp.dot(
                toks[j], up[:, start : start + size], preferred_element_type=jnp.float32
            )
            value = value * jax.nn.sigmoid(value)
            hid[j, :, pl.ds(pl.multiple_of(t * width + start, 128), size)] = value.astype(
                jnp.bfloat16
            )

    def shared(buf, cols, sems, j, owner, target):
        view = buf.at[j, :, cols(owner)]
        return remote(view, view, sems, j, tp=target)

    half_rows = capacity // 2

    def item(k, sems, owner, target):
        if isinstance(k, int) and k in (0, n):
            rows = pl.ds(half_rows if k else 0, half_rows)
            view = hid.at[0, rows, h_cols(owner)]
        else:
            view = hid.at[k, :, h_cols(owner)]
        return remote(view, view, sems, k, tp=target)

    def send_item(k):
        item(k, hx, t, across).start()
        item(k, hm, t, mate).start()

    def forward_item(k):
        item(k, hx, across, across).wait_recv()
        item(k, hf, across, mate).start()

    load_up.wait()
    hidden_block(0)
    send_item(0)

    send_halo.wait()
    padded[0:HALO, :] = jnp.where(e > 0, halo[...].astype(jnp.float32), 0.0)
    taps = taps_ref[...].astype(jnp.float32)
    conv = jnp.zeros((length, channels), jnp.float32)
    for k in range(CONV):
        lead = HALO - (CONV - 1) + k
        conv = conv + padded[lead : lead + length, :] * taps[k : k + 1, :]
    conv_half = conv.astype(jnp.bfloat16)
    conv_buf[...] = conv
    blocks, size = carry_w_ref.shape[0], carry_w_ref.shape[1]

    def gate(w_ref):
        whole = jnp.zeros((channels, channels), jnp.float32)
        for b in range(blocks):
            tall = (
                lax.broadcasted_iota(jnp.int32, (channels, size), 0)
                == lax.broadcasted_iota(jnp.int32, (channels, size), 1) + b * size
            )
            wide = (
                lax.broadcasted_iota(jnp.int32, (size, channels), 1)
                == lax.broadcasted_iota(jnp.int32, (size, channels), 0) + b * size
            )
            right = jnp.dot(
                w_ref[b],
                wide.astype(jnp.float32).astype(jnp.bfloat16),
                preferred_element_type=jnp.float32,
            ).astype(jnp.bfloat16)
            whole = whole + jnp.dot(
                tall.astype(jnp.float32).astype(jnp.bfloat16),
                right,
                preferred_element_type=jnp.float32,
            )
        return jax.nn.sigmoid(
            jnp.dot(conv_half, whole.astype(jnp.bfloat16), preferred_element_type=jnp.float32)
        )

    lane = -lane_ref[...].reshape(1, channels)
    soft = jnp.maximum(lane, 0.0) + jnp.log1p(jnp.exp(-jnp.abs(lane)))
    fade = -8.0 * gate(carry_w_ref) * soft + as_column(jump_ref[...])
    state = jnp.sqrt(one_minus_exp(2.0 * fade)) * gate(entry_w_ref) * conv_buf[...]
    decay = jnp.exp(fade)
    place = lax.broadcasted_iota(jnp.int32, (length, channels), 0)
    shift = 1
    while shift < length:
        older_decay = jnp.where(place < shift, 1.0, pltpu.roll(decay, shift, 0))
        older_state = jnp.where(place < shift, 0.0, pltpu.roll(state, shift, 0))
        state = decay * older_state + state
        decay = decay * older_decay
        shift *= 2
    decay_buf[...] = decay
    state_buf[...] = state
    carry_out[0:8, :] = jnp.broadcast_to(decay[length - 1 : length, :], (8, channels))
    carry_out[8:16, :] = jnp.broadcast_to(state[length - 1 : length, :], (8, channels))

    def send_carry(j):
        return remote(carry_out, carry_in.at[j], carry_sems, j, ep=(e + n - j) % n)

    for j in range(1, n):
        send_carry(j).start()

    def first_matmul(j):
        shared(toks, f_cols, tx, j, across, across).wait_recv()
        shared(toks, f_cols, tf, j, across, mate).start()
        shared(toks, f_cols, tm, j, mate, mate).wait_recv()
        shared(toks, f_cols, tf, j, far, mate).wait_recv()
        hidden_block(j)
        send_item(j)

    def spread(j, _):
        @pl.when(j < n)
        def _():
            send_tokens(j).wait_recv()
            shared(toks, f_cols, tx, j, t, across).start()
            shared(toks, f_cols, tm, j, t, mate).start()

        @pl.when(j > 1)
        def _():
            first_matmul(j - 1)

        return 0

    lax.fori_loop(1, n + 1, spread, 0)
    send_item(n)

    entering = jnp.zeros((1, channels), jnp.float32)
    for j in range(1, n):
        send_carry(j).wait_recv()
    for origin in range(n - 1):
        slot = (origin + n - e) % n
        slot = jnp.where(slot == 0, 1, slot)
        early = carry_in[slot]
        after = early[0:1, :] * entering + early[8:9, :]
        entering = jnp.where(origin < e, after, entering)
    gelu_in = valve_ref[...].astype(jnp.float32)
    inner = 0.7978845608028654 * (gelu_in + 0.044715 * (gelu_in * gelu_in * gelu_in))
    gelu = gelu_in * (0.5 * (1.0 + jnp.tanh(inner)))
    final = (state_buf[...] + decay_buf[...] * entering).T
    scan_out[...] = (final * gelu).astype(jnp.bfloat16)

    load_down.wait()
    out_width = down.shape[1]

    def send_back(j):
        return remote(res.at[j], back.at[j], rz, j, ep=(e + j) % n)

    def k_dot(j, rows, first, size):
        cols = pl.ds(pl.multiple_of(first, 128), size)
        return jnp.dot(hid[j, rows, cols], down[cols, :], preferred_element_type=jnp.float32)

    def second_matmul(k, j, rows, size):
        item(k, hm, mate, mate).wait_recv()
        acc[0:size, :] = k_dot(j, rows, (t // 2) * 2 * width, 2 * width)
        forward_item(k)
        acc[0:size, :] += k_dot(j, rows, across * width, width)
        item(k, hf, far, mate).wait_recv()
        res[j, rows, :] = (acc[0:size, :] + k_dot(j, rows, far * width, width)).astype(
            jnp.bfloat16
        )

    def second_block(j, _):
        second_matmul(j, j, pl.ds(0, capacity), capacity)
        send_back(j).start()
        return 0

    second_matmul(0, 0, pl.ds(0, half_rows), half_rows)
    lax.fori_loop(1, n, second_block, 0)
    second_matmul(n, 0, pl.ds(half_rows, half_rows), half_rows)

    first_col, second_col = as_column(first), as_column(second)
    scores = score_ref[...]
    first_weight = jax.nn.sigmoid(as_column(scores[0:1, :] - scores[1:2, :]))
    slots = lax.broadcasted_iota(jnp.int32, (tokens, capacity), 1).astype(jnp.float32)
    total = jnp.zeros((tokens, out_width), jnp.float32)
    for j in [*range(1, n - 1), 0, n - 1]:
        expert = (e + n - j) % n
        number = expert.astype(jnp.float32)
        rank_col = as_column(rank_rows[pl.ds(expert, 1), :])
        chosen = (slots == rank_col).astype(jnp.float32).astype(jnp.bfloat16)
        weight = jnp.where(first_col == number, first_weight, 0.0) + jnp.where(
            second_col == number, 1.0 - first_weight, 0.0
        )
        if j > 0:
            send_back(j).wait_recv()
        source = res[0] if j == 0 else back[j]
        total = total + weight * jnp.dot(chosen, source, preferred_element_type=jnp.float32)
    moe_out[...] = total.astype(jnp.bfloat16)

    def drain(j, _):
        send_tokens(j).wait_send()
        send_carry(j).wait_send()
        send_back(j).wait_send()
        shared(toks, f_cols, tx, j, t, across).wait_send()
        shared(toks, f_cols, tm, j, t, mate).wait_send()
        shared(toks, f_cols, tf, j, across, mate).wait_send()
        return 0

    lax.fori_loop(1, n, drain, 0)

    def drain_item(k):
        item(k, hx, t, across).wait_send()
        item(k, hm, t, mate).wait_send()
        item(k, hf, across, mate).wait_send()

    def drain_block(j, _):
        drain_item(j)
        return 0

    drain_item(0)
    lax.fori_loop(1, n, drain_block, 0)
    drain_item(n)


def slots_per_expert(tokens, top_count, experts, tp_size):
    return tp_size * ((3 * tokens * top_count + 2 * experts * tp_size - 1) // (2 * experts * tp_size))


def fused(*arrays):
    (scan, valve, taps, carry_w, entry_w, lane, jump, tok, gain, routes, scores, up, down) = arrays
    n = lax.axis_size("ep")
    length, channels = scan.shape
    tokens, features = tok.shape
    width, out_width = up.shape[2], down.shape[2]
    units = down.shape[1]
    capacity = slots_per_expert(tokens, routes.shape[1], n, lax.axis_size("tp"))
    half, full = jnp.bfloat16, jnp.float32
    vmem = pl.BlockSpec(memory_space=pltpu.VMEM)
    hbm = pl.BlockSpec(memory_space=pl.ANY)
    pair = pltpu.SemaphoreType.DMA((2, n))
    turned, moe = pl.pallas_call(
        functools.partial(fused_kernel, n, capacity),
        out_shape=(
            jax.ShapeDtypeStruct((channels, length), half),
            jax.ShapeDtypeStruct((tokens, out_width), half),
        ),
        in_specs=[vmem] * 11 + [hbm] * 2,
        out_specs=(vmem, vmem),
        scratch_shapes=[
            pltpu.VMEM((features, width), half),
            pltpu.VMEM((units, out_width), half),
            pltpu.VMEM((tokens, features), half),
            pltpu.VMEM((-(-n // 8) * 8, tokens), full),
            pltpu.VMEM((n, capacity, features // 4), half),
            pltpu.VMEM((n, capacity, features), half),
            pltpu.VMEM((n, capacity, units), half),
            pltpu.VMEM((n, capacity, out_width), half),
            pltpu.VMEM((n, capacity, out_width), half),
            pltpu.VMEM((HALO, channels), half),
            pltpu.VMEM((length + HALO, channels), full),
            pltpu.VMEM((length, channels), full),
            pltpu.VMEM((length, channels), full),
            pltpu.VMEM((length, channels), full),
            pltpu.VMEM((16, channels), full),
            pltpu.VMEM((n, 16, channels), full),
            pltpu.VMEM((HALO, channels), half),
            pltpu.VMEM((capacity, out_width), full),
            pltpu.SemaphoreType.DMA((2,)),
            *([pair] * 4),
            *([pltpu.SemaphoreType.DMA((2, n + 1))] * 3),
            pair,
            pltpu.SemaphoreType.DMA((2, 1)),
            pair,
        ],
        compiler_params=pltpu.CompilerParams(
            collective_id=0, has_side_effects=True, vmem_limit_bytes=60 * 1024 * 1024
        ),
    )(
        scan.T,
        valve.T,
        taps,
        carry_w,
        entry_w,
        lane,
        jump.reshape(1, -1),
        tok,
        gain.reshape(1, -1),
        routes.T,
        scores.T,
        up,
        down,
    )
    return turned.T, moe


def fits_fused(tok, routes, up, down):
    n, tp_size = lax.axis_size("ep"), lax.axis_size("tp")
    if tp_size != 4 or n < 2 or up.shape[0] != 1 or routes.shape[1] != 2:
        return False
    capacity = slots_per_expert(tok.shape[0], 2, n, tp_size)
    if capacity % 32 or tok.shape[0] % 32 or up.shape[2] % 128 or down.shape[2] % 256:
        return False
    held = n * capacity * (tok.shape[1] + down.shape[1] + 4 * down.shape[2])
    return 2 * (held + up.size + down.size + 2 * tok.size) < 40 * 1024 * 1024


def on_device(
    scan_branch_source,
    valve_branch_source,
    stencil_factors,
    carry_valve_matrix,
    entry_valve_matrix,
    lane_fade_param,
    jump_log_fade,
    specialist_entries,
    specialist_rms_scale,
    assigned_specialists,
    picked_route_scores,
    expand_matrix,
    contract_matrix,
):
    if fits_fused(specialist_entries, assigned_specialists, expand_matrix, contract_matrix):
        return fused(
            scan_branch_source,
            valve_branch_source,
            stencil_factors,
            carry_valve_matrix,
            entry_valve_matrix,
            lane_fade_param,
            jump_log_fade,
            specialist_entries,
            specialist_rms_scale,
            assigned_specialists,
            picked_route_scores,
            expand_matrix,
            contract_matrix,
        )
    valved_scan_target = temporal_block_part(
        scan_branch_source,
        valve_branch_source,
        stencil_factors,
        carry_valve_matrix,
        entry_valve_matrix,
        lane_fade_param,
        jump_log_fade,
    )
    moe_out = expert_part(
        specialist_entries,
        specialist_rms_scale,
        assigned_specialists,
        picked_route_scores,
        expand_matrix,
        contract_matrix,
    )
    return (valved_scan_target, moe_out)


def solution(mesh):
    placed = (
        P(("grp", "ep"), "tp"),
        P(("grp", "ep"), "tp"),
        P(None, "tp"),
        P("tp", None, None),
        P("tp", None, None),
        P("tp"),
        P(("grp", "ep")),
        P(("grp", "ep"), None),
        P(),
        P(("grp", "ep"), None),
        P(("grp", "ep"), None),
        P("ep", None, "tp"),
        P("ep", None, "tp"),
    )
    return jax.shard_map(
        on_device,
        mesh=mesh,
        in_specs=placed,
        out_specs=(P(("grp", "ep"), "tp"), P(("grp", "ep"), "tp")),
        check_vma=False,
    )
```

profile of v0, /device:TPU:0, one launch (start us, length us, event | category | flops | bytes accessed | tf_op | source)
XLA Modules:
  0.0 70.7 jit_solution(2533290969134360495)
XLA Ops:
  0.6 66.9 %shard_map.140 = (bf16[336,128]{1,0:T(8,128)(2,1)}, bf16[256,512]{1,0:T(8,128)(2,1)}) custom-call(bf16[336,128]{1,0:T(8,128)(2,1)} %bitcast.8, bf16[336,128]{1,0:T(8,128)(2,1)} %bitcast.9, bf16[4,336]{1,0:T(4,128)(2,1)} %taps_ref.1, bf16[2,168,168]{2,1,0:T(8,128)(2,1)} %carry_w_ref.1, bf16[2,168,168]{2,1,0:T(8,128)(2,1)} %entry_w_ref.1, f32[336]{0:T(512)} %lane_ref.1, ...), custom_call_target="tpu_custom_call" | custom-call | tf_op jit(solution)/shard_map/pallas_call | solution.py:539
  67.5 1.5 %copy.17 = bf16[128,336]{0,1:T(8,128)(2,1)} copy(bf16[128,336]{0,1:T(8,128)(2,1)} %bitcast.7) | data formatting | bytes 172032
  69.1 1.7 %copy.18 = bf16[256,512]{1,0:T(8,128)(2,1)} copy(bf16[256,512]{1,0:T(8,128)(2,1)} %get-tuple-element.9) | data formatting | bytes 524288
where the time goes:
time: 71 us; the launch traced here: 70.7 us
  Pallas kernels  66.9 us (94%)
  local copies, waits for them, and re-layouts  3.2 us (5%)
    pallas_call x1, Pallas kernels, fused(): pl.pallas_call(functools.partial(fused_kernel, n, capacity), out_shape=(j...  66.9 us
    unnamed x2, local copies, waits for them, and re-layouts  3.2 us

commit v1 on v0

--- a/solution.py
+++ b/solution.py
@@ -179,6 +179,18 @@
     return jnp.where(x > -0.35, -near * series, 1.0 - jnp.exp(x))
 
 
+OWN, NEAR, INNER, OUTER = 0, 1, 2, 3
+PARTS = {OWN: 3, NEAR: 3, INNER: 3, OUTER: 3}
+ORDER = (
+    "D31", "D21", "D32", "P01", "D13", "T31", "P02", "F31", "T21", "D22", "D11", "M31",
+    "T22", "T13", "F13", "F21", "D33", "T11", "D23", "F11", "T32", "D12", "M21", "F22",
+    "T33", "F32", "M32", "G31", "M22", "T23", "S31", "A", "T12", "F12", "F33", "M33",
+    "M11", "G32", "G21", "G01", "M12", "F23", "S32", "M23", "M13", "S21", "G33", "S33",
+    "P03", "G11", "G22", "S11", "S22", "B", "G12", "S12", "G02", "G23", "S23", "G13",
+    "S13", "G03", "S01", "S03", "S02", "C0", "C2", "C3", "C1",
+)
+
+
 def fused_kernel(
     n,
     capacity,
@@ -201,11 +213,16 @@
     down,
     normed,
     rank_rows,
-    out_rows,
+    near_rows,
+    cross_rows,
     toks,
     hid,
     res,
     back,
+    acc,
+    chosen,
+    share,
+    total,
     halo,
     padded,
     conv_buf,
@@ -214,7 +231,6 @@
     carry_out,
     carry_in,
     halo_out,
-    acc,
     load_sems,
     zt,
     tx,
@@ -232,15 +248,27 @@
     mate = t + 1 - 2 * (t % 2)
     across = (t + 2) % 4
     far = (mate + 2) % 4
+    upper = e // 2
+    peer = {NEAR: e + 1 - 2 * (e % 2), INNER: 2 - upper, OUTER: 3 - 3 * upper}
+    cross_slot = OUTER - (e + upper) % 2
+    slot_there = {NEAR: NEAR, INNER: cross_slot, OUTER: cross_slot}
     tokens, features = tok_ref.shape
     part = features // 4
     width = up.shape[1]
+    out_width = down.shape[1]
 
     def f_cols(i):
         return pl.ds(pl.multiple_of(i * part, part), part)
 
+    def half_cols(i):
+        return pl.ds(pl.multiple_of((i % 2) * 2 * part, 2 * part), 2 * part)
+
     def h_cols(i):
         return pl.ds(pl.multiple_of(i * width, 128), width)
+
+    def piece(slot, c):
+        size = capacity // PARTS[slot]
+        return pl.ds(c * size, size)
 
     barrier = pltpu.get_barrier_semaphore()
     for j in range(1, n):
@@ -252,11 +280,13 @@
     load_up.start()
     load_down.start()
     channels, length = scan_ref.shape
-    turned = scan_ref[...].astype(jnp.float32).T
-    padded[HALO:, :] = turned
-    halo_out[...] = turned[length - HALO :, :].astype(jnp.bfloat16)
-
-    rows_step = 32
+
+    with jax.named_scope("halo_prep"):
+        turned = scan_ref[...].astype(jnp.float32).T
+        padded[HALO:, :] = turned
+        halo_out[...] = turned[length - HALO :, :].astype(jnp.bfloat16)
+
+    rows_step = 64
 
     def norm_rows(i, _):
         rows = pl.ds(pl.multiple_of(i * rows_step, rows_step), rows_step)
@@ -266,109 +296,200 @@
         normed[rows, :] = (centered * lax.rsqrt(var + 1e-05) * gain_ref[...]).astype(jnp.bfloat16)
         return 0
 
-    lax.fori_loop(0, tokens // rows_step, norm_rows, 0)
-
-    routes = route_ref[...].astype(jnp.float32)
-    first, second = routes[0:1, :], routes[1:2, :]
-    erow = lax.broadcasted_iota(jnp.int32, (rank_rows.shape[0], tokens), 0).astype(jnp.float32)
-    hit = (erow == first) | (erow == second)
-    ti = lax.broadcasted_iota(jnp.int32, (tokens, tokens), 0)
-    tj = lax.broadcasted_iota(jnp.int32, (tokens, tokens), 1)
-    rank = jnp.dot(
-        hit.astype(jnp.float32).astype(jnp.bfloat16),
-        (ti < tj).astype(jnp.float32).astype(jnp.bfloat16),
-        preferred_element_type=jnp.float32,
-    )
-    rank_rows[...] = jnp.where(hit, rank, -1.0)
-
-    def picker(expert):
-        slots = lax.broadcasted_iota(jnp.int32, (capacity, tokens), 0).astype(jnp.float32)
-        chosen = slots == rank_rows[pl.ds(expert, 1), :]
-        return chosen.astype(jnp.float32).astype(jnp.bfloat16)
-
-    pl.semaphore_wait(barrier, n + 1)
+    with jax.named_scope("norm"):
+        lax.fori_loop(0, tokens // rows_step, norm_rows, 0)
+
+    with jax.named_scope("rank"):
+        routes = route_ref[...].astype(jnp.float32)
+        first, second = routes[0:1, :], routes[1:2, :]
+        erow = lax.broadcasted_iota(jnp.int32, (rank_rows.shape[0], tokens), 0).astype(jnp.float32)
+        hit = (erow == first) | (erow == second)
+        ti = lax.broadcasted_iota(jnp.int32, (tokens, tokens), 0)
+        tj = lax.broadcasted_iota(jnp.int32, (tokens, tokens), 1)
+        rank = jnp.dot(
+            hit.astype(jnp.float32).astype(jnp.bfloat16),
+            (ti < tj).astype(jnp.float32).astype(jnp.bfloat16),
+            preferred_element_type=jnp.float32,
+        )
+        rank_rows[...] = jnp.where(hit, rank, -1.0)
+
+    def picker(expert, start, size):
+        slots = start + lax.broadcasted_iota(jnp.int32, (size, tokens), 0)
+        hits = slots.astype(jnp.float32) == rank_rows[pl.ds(expert, 1), :]
+        return hits.astype(jnp.float32).astype(jnp.bfloat16)
+
+    with jax.named_scope("barrier"):
+        pl.semaphore_wait(barrier, n + 1)
 
     send_halo = remote(halo_out, halo, halo_sems, 0, ep=(e + 1) % n)
     send_halo.start()
-
-    def send_tokens(j):
-        return remote(
-            out_rows.at[j], toks.at[j, :, f_cols(t)], zt, j, ep=(e + n - j) % n
-        )
-
-    def dispatch(j, _):
-        out_rows[j] = jnp.dot(
-            picker((e + n - j) % n), normed[:, f_cols(t)], preferred_element_type=jnp.float32
-        ).astype(jnp.bfloat16)
-        send_tokens(j).start()
-        return 0
-
-    lax.fori_loop(1, n, dispatch, 0)
-
-    mine = picker(e)
-    for q in range(4):
-        toks[0, :, q * part : (q + 1) * part] = jnp.dot(
-            mine, normed[:, q * part : (q + 1) * part], preferred_element_type=jnp.float32
-        ).astype(jnp.bfloat16)
-
-    def hidden_block(j):
+    sent = [send_halo]
+    waited = []
+
+    def begin(copy):
+        copy.start()
+        sent.append(copy)
+
+    def token_copy(role, c):
+        rows = piece(role, c)
+        if role == NEAR:
+            origin, cols = near_rows.at[rows], half_cols(t)
+        else:
+            origin, cols = cross_rows.at[role - INNER, rows], f_cols(t)
+        slot = slot_there[role]
+        return pltpu.make_async_remote_copy(
+            src_ref=origin,
+            dst_ref=toks.at[slot, rows, cols],
+            send_sem=zt.at[0, role, c],
+            recv_sem=zt.at[1, slot, c],
+            device_id={"ep": peer[role]},
+            device_id_type=MESH,
+        )
+
+    def token_arrival(slot, c):
+        rows = piece(slot, c)
+        cols = half_cols(t) if slot == NEAR else f_cols(t)
+        view = toks.at[slot, rows, cols]
+        return pltpu.make_async_remote_copy(
+            src_ref=view,
+            dst_ref=view,
+            send_sem=zt.at[0, slot, c],
+            recv_sem=zt.at[1, slot, c],
+            device_id={"ep": peer[slot]},
+            device_id_type=MESH,
+        )
+
+    def shared(view, sems, slot, c, target):
+        return pltpu.make_async_remote_copy(
+            src_ref=view,
+            dst_ref=view,
+            send_sem=sems.at[0, slot, c],
+            recv_sem=sems.at[1, slot, c],
+            device_id={"tp": target},
+            device_id_type=MESH,
+        )
+
+    def tok_view(slot, c, owner):
+        cols = half_cols(owner) if slot == NEAR else f_cols(owner)
+        return toks.at[slot, piece(slot, c), cols]
+
+    def hid_view(slot, c, owner):
+        return hid.at[slot, piece(slot, c), h_cols(owner)]
+
+    def result_copy(slot, c):
+        rows = piece(slot, c)
+        there = slot_there[slot]
+        return pltpu.make_async_remote_copy(
+            src_ref=res.at[slot, rows],
+            dst_ref=back.at[there, rows],
+            send_sem=rz.at[0, slot, c],
+            recv_sem=rz.at[1, there, c],
+            device_id={"ep": peer[slot]},
+            device_id_type=MESH,
+        )
+
+    def result_arrival(role, c):
+        view = back.at[role, piece(role, c)]
+        return pltpu.make_async_remote_copy(
+            src_ref=view,
+            dst_ref=view,
+            send_sem=rz.at[0, role, c],
+            recv_sem=rz.at[1, role, c],
+            device_id={"ep": peer[role]},
+            device_id_type=MESH,
+        )
+
+    def dispatch(role, c):
+        size = capacity // PARTS[role]
+        pick = picker(peer[role], c * size, size)
+        if role == NEAR:
+            picked = jnp.dot(pick, normed[:, half_cols(t)], preferred_element_type=jnp.float32)
+            near_rows[piece(role, c), :] = picked.astype(jnp.bfloat16)
+        else:
+            picked = jnp.dot(pick, normed[:, f_cols(t)], preferred_element_type=jnp.float32)
+            cross_rows[role - INNER, piece(role, c), :] = picked.astype(jnp.bfloat16)
+        begin(token_copy(role, c))
+
+    def first_matmul(slot, c):
+        rows = piece(slot, c)
         for start in range(0, width, 256):
             size = min(256, width - start)
             value = jnp.dot(
-                toks[j], up[:, start : start + size], preferred_element_type=jnp.float32
+                toks[slot, rows, :],
+                up[:, start : start + size],
+                preferred_element_type=jnp.float32,
             )
             value = value * jax.nn.sigmoid(value)
-            hid[j, :, pl.ds(pl.multiple_of(t * width + start, 128), size)] = value.astype(
-                jnp.bfloat16
-            )
-
-    def shared(buf, cols, sems, j, owner, target):
-        view = buf.at[j, :, cols(owner)]
-        return remote(view, view, sems, j, tp=target)
-
-    half_rows = capacity // 2
-
-    def item(k, sems, owner, target):
-        if isinstance(k, int) and k in (0, n):
-            rows = pl.ds(half_rows if k else 0, half_rows)
-            view = hid.at[0, rows, h_cols(owner)]
-        else:
-            view = hid.at[k, :, h_cols(owner)]
-        return remote(view, view, sems, k, tp=target)
-
-    def send_item(k):
-        item(k, hx, t, across).start()
-        item(k, hm, t, mate).start()
-
-    def forward_item(k):
-        item(k, hx, across, across).wait_recv()
-        item(k, hf, across, mate).start()
-
-    load_up.wait()
-    hidden_block(0)
-    send_item(0)
-
-    send_halo.wait()
-    padded[0:HALO, :] = jnp.where(e > 0, halo[...].astype(jnp.float32), 0.0)
-    taps = taps_ref[...].astype(jnp.float32)
-    conv = jnp.zeros((length, channels), jnp.float32)
-    for k in range(CONV):
-        lead = HALO - (CONV - 1) + k
-        conv = conv + padded[lead : lead + length, :] * taps[k : k + 1, :]
-    conv_half = conv.astype(jnp.bfloat16)
-    conv_buf[...] = conv
-    blocks, size = carry_w_ref.shape[0], carry_w_ref.shape[1]
-
-    def gate(w_ref):
+            cols = pl.ds(pl.multiple_of(t * width + start, 128), size)
+            hid[slot, rows, cols] = value.astype(jnp.bfloat16)
+        begin(shared(hid_view(slot, c, t), hx, slot, c, across))
+        begin(shared(hid_view(slot, c, t), hm, slot, c, mate))
+
+    def own_tokens(_, c):
+        size = capacity // PARTS[OWN]
+        mine = picker(e, c * size, size)
+        for q in range(4):
+            cols = slice(q * part, (q + 1) * part)
+            picked = jnp.dot(mine, normed[:, cols], preferred_element_type=jnp.float32)
+            toks[OWN, piece(OWN, c), cols] = picked.astype(jnp.bfloat16)
+        if "up" not in waited:
+            load_up.wait()
+            waited.append("up")
+        first_matmul(OWN, c)
+
+    def spread(slot, c):
+        token_arrival(slot, c).wait_recv()
+        begin(shared(tok_view(slot, c, t), tm, slot, c, mate))
+        if slot != NEAR:
+            begin(shared(tok_view(slot, c, t), tx, slot, c, across))
+
+    def forward(slot, c):
+        if slot != NEAR:
+            shared(tok_view(slot, c, across), tx, slot, c, across).wait_recv()
+            begin(shared(tok_view(slot, c, across), tf, slot, c, mate))
+
+    def hidden_block(slot, c):
+        shared(tok_view(slot, c, mate), tm, slot, c, mate).wait_recv()
+        if slot != NEAR:
+            shared(tok_view(slot, c, far), tf, slot, c, mate).wait_recv()
+        first_matmul(slot, c)
+
+    def k_dot(slot, rows, first_row, size):
+        cols = pl.ds(pl.multiple_of(first_row, 128), size)
+        return jnp.dot(hid[slot, rows, cols], down[cols, :], preferred_element_type=jnp.float32)
+
+    def gather_block(slot, c):
+        rows = piece(slot, c)
+        shared(hid_view(slot, c, across), hx, slot, c, across).wait_recv()
+        begin(shared(hid_view(slot, c, across), hf, slot, c, mate))
+        shared(hid_view(slot, c, mate), hm, slot, c, mate).wait_recv()
+        if "down" not in waited:
+            load_down.wait()
+            waited.append("down")
+        local = k_dot(slot, rows, (t // 2) * 2 * width, 2 * width)
+        acc[slot, rows, :] = local + k_dot(slot, rows, across * width, width)
+
+    def finish_block(slot, c):
+        rows = piece(slot, c)
+        shared(hid_view(slot, c, far), hf, slot, c, mate).wait_recv()
+        res[slot, rows, :] = (acc[slot, rows, :] + k_dot(slot, rows, far * width, width)).astype(
+            jnp.bfloat16
+        )
+        if slot != OWN:
+            begin(result_copy(slot, c))
+
+    blocks, size_w = carry_w_ref.shape[0], carry_w_ref.shape[1]
+
+    def gate(w_ref, conv_half):
         whole = jnp.zeros((channels, channels), jnp.float32)
         for b in range(blocks):
             tall = (
-                lax.broadcasted_iota(jnp.int32, (channels, size), 0)
-                == lax.broadcasted_iota(jnp.int32, (channels, size), 1) + b * size
+                lax.broadcasted_iota(jnp.int32, (channels, size_w), 0)
+                == lax.broadcasted_iota(jnp.int32, (channels, size_w), 1) + b * size_w
             )
             wide = (
-                lax.broadcasted_iota(jnp.int32, (size, channels), 1)
-                == lax.broadcasted_iota(jnp.int32, (size, channels), 0) + b * size
+                lax.broadcasted_iota(jnp.int32, (size_w, channels), 1)
+                == lax.broadcasted_iota(jnp.int32, (size_w, channels), 0) + b * size_w
             )
             right = jnp.dot(
                 w_ref[b],
@@ -384,140 +505,111 @@
             jnp.dot(conv_half, whole.astype(jnp.bfloat16), preferred_element_type=jnp.float32)
         )
 
-    lane = -lane_ref[...].reshape(1, channels)
-    soft = jnp.maximum(lane, 0.0) + jnp.log1p(jnp.exp(-jnp.abs(lane)))
-    fade = -8.0 * gate(carry_w_ref) * soft + as_column(jump_ref[...])
-    state = jnp.sqrt(one_minus_exp(2.0 * fade)) * gate(entry_w_ref) * conv_buf[...]
-    decay = jnp.exp(fade)
-    place = lax.broadcasted_iota(jnp.int32, (length, channels), 0)
-    shift = 1
-    while shift < length:
-        older_decay = jnp.where(place < shift, 1.0, pltpu.roll(decay, shift, 0))
-        older_state = jnp.where(place < shift, 0.0, pltpu.roll(state, shift, 0))
-        state = decay * older_state + state
-        decay = decay * older_decay
-        shift *= 2
-    decay_buf[...] = decay
-    state_buf[...] = state
-    carry_out[0:8, :] = jnp.broadcast_to(decay[length - 1 : length, :], (8, channels))
-    carry_out[8:16, :] = jnp.broadcast_to(state[length - 1 : length, :], (8, channels))
-
-    def send_carry(j):
+    def carry_copy(j):
         return remote(carry_out, carry_in.at[j], carry_sems, j, ep=(e + n - j) % n)
 
-    for j in range(1, n):
-        send_carry(j).start()
-
-    def first_matmul(j):
-        shared(toks, f_cols, tx, j, across, across).wait_recv()
-        shared(toks, f_cols, tf, j, across, mate).start()
-        shared(toks, f_cols, tm, j, mate, mate).wait_recv()
-        shared(toks, f_cols, tf, j, far, mate).wait_recv()
-        hidden_block(j)
-        send_item(j)
-
-    def spread(j, _):
-        @pl.when(j < n)
-        def _():
-            send_tokens(j).wait_recv()
-            shared(toks, f_cols, tx, j, t, across).start()
-            shared(toks, f_cols, tm, j, t, mate).start()
-
-        @pl.when(j > 1)
-        def _():
-            first_matmul(j - 1)
-
-        return 0
-
-    lax.fori_loop(1, n + 1, spread, 0)
-    send_item(n)
-
-    entering = jnp.zeros((1, channels), jnp.float32)
-    for j in range(1, n):
-        send_carry(j).wait_recv()
-    for origin in range(n - 1):
-        slot = (origin + n - e) % n
-        slot = jnp.where(slot == 0, 1, slot)
-        early = carry_in[slot]
-        after = early[0:1, :] * entering + early[8:9, :]
-        entering = jnp.where(origin < e, after, entering)
-    gelu_in = valve_ref[...].astype(jnp.float32)
-    inner = 0.7978845608028654 * (gelu_in + 0.044715 * (gelu_in * gelu_in * gelu_in))
-    gelu = gelu_in * (0.5 * (1.0 + jnp.tanh(inner)))
-    final = (state_buf[...] + decay_buf[...] * entering).T
-    scan_out[...] = (final * gelu).astype(jnp.bfloat16)
-
-    load_down.wait()
-    out_width = down.shape[1]
-
-    def send_back(j):
-        return remote(res.at[j], back.at[j], rz, j, ep=(e + j) % n)
-
-    def k_dot(j, rows, first, size):
-        cols = pl.ds(pl.multiple_of(first, 128), size)
-        return jnp.dot(hid[j, rows, cols], down[cols, :], preferred_element_type=jnp.float32)
-
-    def second_matmul(k, j, rows, size):
-        item(k, hm, mate, mate).wait_recv()
-        acc[0:size, :] = k_dot(j, rows, (t // 2) * 2 * width, 2 * width)
-        forward_item(k)
-        acc[0:size, :] += k_dot(j, rows, across * width, width)
-        item(k, hf, far, mate).wait_recv()
-        res[j, rows, :] = (acc[0:size, :] + k_dot(j, rows, far * width, width)).astype(
-            jnp.bfloat16
-        )
-
-    def second_block(j, _):
-        second_matmul(j, j, pl.ds(0, capacity), capacity)
-        send_back(j).start()
-        return 0
-
-    second_matmul(0, 0, pl.ds(0, half_rows), half_rows)
-    lax.fori_loop(1, n, second_block, 0)
-    second_matmul(n, 0, pl.ds(half_rows, half_rows), half_rows)
-
-    first_col, second_col = as_column(first), as_column(second)
-    scores = score_ref[...]
-    first_weight = jax.nn.sigmoid(as_column(scores[0:1, :] - scores[1:2, :]))
-    slots = lax.broadcasted_iota(jnp.int32, (tokens, capacity), 1).astype(jnp.float32)
-    total = jnp.zeros((tokens, out_width), jnp.float32)
-    for j in [*range(1, n - 1), 0, n - 1]:
-        expert = (e + n - j) % n
-        number = expert.astype(jnp.float32)
-        rank_col = as_column(rank_rows[pl.ds(expert, 1), :])
-        chosen = (slots == rank_col).astype(jnp.float32).astype(jnp.bfloat16)
-        weight = jnp.where(first_col == number, first_weight, 0.0) + jnp.where(
-            second_col == number, 1.0 - first_weight, 0.0
-        )
-        if j > 0:
-            send_back(j).wait_recv()
-        source = res[0] if j == 0 else back[j]
-        total = total + weight * jnp.dot(chosen, source, preferred_element_type=jnp.float32)
-    moe_out[...] = total.astype(jnp.bfloat16)
-
-    def drain(j, _):
-        send_tokens(j).wait_send()
-        send_carry(j).wait_send()
-        send_back(j).wait_send()
-        shared(toks, f_cols, tx, j, t, across).wait_send()
-        shared(toks, f_cols, tm, j, t, mate).wait_send()
-        shared(toks, f_cols, tf, j, across, mate).wait_send()
-        return 0
-
-    lax.fori_loop(1, n, drain, 0)
-
-    def drain_item(k):
-        item(k, hx, t, across).wait_send()
-        item(k, hm, t, mate).wait_send()
-        item(k, hf, across, mate).wait_send()
-
-    def drain_block(j, _):
-        drain_item(j)
-        return 0
-
-    drain_item(0)
-    lax.fori_loop(1, n, drain_block, 0)
-    drain_item(n)
+    def scan_local():
+        send_halo.wait_recv()
+        padded[0:HALO, :] = jnp.where(e > 0, halo[...].astype(jnp.float32), 0.0)
+        taps = taps_ref[...].astype(jnp.float32)
+        conv = jnp.zeros((length, channels), jnp.float32)
+        for k in range(CONV):
+            lead = HALO - (CONV - 1) + k
+            conv = conv + padded[lead : lead + length, :] * taps[k : k + 1, :]
+        conv_half = conv.astype(jnp.bfloat16)
+        conv_buf[...] = conv
+        lane = -lane_ref[...].reshape(1, channels)
+        soft = jnp.maximum(lane, 0.0) + jnp.log1p(jnp.exp(-jnp.abs(lane)))
+        fade = -8.0 * gate(carry_w_ref, conv_half) * soft + as_column(jump_ref[...])
+        state = jnp.sqrt(one_minus_exp(2.0 * fade)) * gate(entry_w_ref, conv_half) * conv_buf[...]
+        decay = jnp.exp(fade)
+        place = lax.broadcasted_iota(jnp.int32, (length, channels), 0)
+        shift = 1
+        while shift < length:
+            older_decay = jnp.where(place < shift, 1.0, pltpu.roll(decay, shift, 0))
+            older_state = jnp.where(place < shift, 0.0, pltpu.roll(state, shift, 0))
+            state = decay * older_state + state
+            decay = decay * older_decay
+            shift *= 2
+        decay_buf[...] = decay
+        state_buf[...] = state
+        carry_out[0:8, :] = jnp.broadcast_to(decay[length - 1 : length, :], (8, channels))
+        carry_out[8:16, :] = jnp.broadcast_to(state[length - 1 : length, :], (8, channels))
+        for j in range(1, n):
+            begin(carry_copy(j))
+
+    def scan_finish():
+        entering = jnp.zeros((1, channels), jnp.float32)
+        for j in range(1, n):
+            carry_copy(j).wait_recv()
+        for origin in range(n - 1):
+            slot = (origin + n - e) % n
+            slot = jnp.where(slot == 0, 1, slot)
+            early = carry_in[slot]
+            after = early[0:1, :] * entering + early[8:9, :]
+            entering = jnp.where(origin < e, after, entering)
+        gelu_in = valve_ref[...].astype(jnp.float32)
+        inner = 0.7978845608028654 * (gelu_in + 0.044715 * (gelu_in * gelu_in * gelu_in))
+        gelu = gelu_in * (0.5 * (1.0 + jnp.tanh(inner)))
+        final = (state_buf[...] + decay_buf[...] * entering).T
+        scan_out[...] = (final * gelu).astype(jnp.bfloat16)
+
+    def plan_combine():
+        first_col, second_col = as_column(first), as_column(second)
+        scores = score_ref[...]
+        first_weight = jax.nn.sigmoid(as_column(scores[0:1, :] - scores[1:2, :]))
+        slots = lax.broadcasted_iota(jnp.int32, (tokens, capacity), 1).astype(jnp.float32)
+        for role in (OWN, NEAR, INNER, OUTER):
+            expert = peer.get(role, e)
+            number = expert.astype(jnp.float32)
+            rank_col = as_column(rank_rows[pl.ds(expert, 1), :])
+            chosen[role] = (slots == rank_col).astype(jnp.float32).astype(jnp.bfloat16)
+            weight = jnp.where(first_col == number, first_weight, 0.0) + jnp.where(
+                second_col == number, 1.0 - first_weight, 0.0
+            )
+            share[role] = jnp.broadcast_to(weight, (tokens, 128))
+
+    added = []
+
+    def combine(role):
+        if role != OWN:
+            for c in range(PARTS[role]):
+                result_arrival(role, c).wait_recv()
+        source = res[OWN] if role == OWN else back[role]
+        term = jnp.dot(chosen[role], source, preferred_element_type=jnp.float32)
+        term = term * jnp.tile(share[role], (1, out_width // 128))
+        if added:
+            term = total[...] + term
+        added.append(role)
+        if len(added) == n:
+            moe_out[...] = term.astype(jnp.bfloat16)
+        else:
+            total[...] = term
+
+    tasks = {
+        "D": dispatch,
+        "P": own_tokens,
+        "T": spread,
+        "F": forward,
+        "M": hidden_block,
+        "G": gather_block,
+        "S": finish_block,
+    }
+    for name in ORDER:
+        with jax.named_scope(name):
+            if name == "A":
+                scan_local()
+            elif name == "B":
+                scan_finish()
+                plan_combine()
+            elif name[0] == "C":
+                combine(int(name[1]))
+            else:
+                tasks[name[0]](int(name[1]), int(name[2]) - 1)
+
+    with jax.named_scope("drain"):
+        for copy in sent:
+            copy.wait_send()
 
 
 def slots_per_expert(tokens, top_count, experts, tp_size):
@@ -536,11 +628,12 @@
     vmem = pl.BlockSpec(memory_space=pltpu.VMEM)
     hbm = pl.BlockSpec(memory_space=pl.ANY)
     pair = pltpu.SemaphoreType.DMA((2, n))
+    pieces = pltpu.SemaphoreType.DMA((2, n, max(PARTS.values())))
     turned, moe = pl.pallas_call(
         functools.partial(fused_kernel, n, capacity),
         out_shape=(
-            jax.ShapeDtypeStruct((channels, length), half),
-            jax.ShapeDtypeStruct((tokens, out_width), half),
+            pltpu.VMEM((channels, length), half),
+            pltpu.VMEM((tokens, out_width), half),
         ),
         in_specs=[vmem] * 11 + [hbm] * 2,
         out_specs=(vmem, vmem),
@@ -549,11 +642,16 @@
             pltpu.VMEM((units, out_width), half),
             pltpu.VMEM((tokens, features), half),
             pltpu.VMEM((-(-n // 8) * 8, tokens), full),
-            pltpu.VMEM((n, capacity, features // 4), half),
+            pltpu.VMEM((capacity, features // 2), half),
+            pltpu.VMEM((2, capacity, features // 4), half),
             pltpu.VMEM((n, capacity, features), half),
             pltpu.VMEM((n, capacity, units), half),
             pltpu.VMEM((n, capacity, out_width), half),
             pltpu.VMEM((n, capacity, out_width), half),
+            pltpu.VMEM((n, capacity, out_width), full),
+            pltpu.VMEM((n, tokens, capacity), half),
+            pltpu.VMEM((n, tokens, 128), full),
+            pltpu.VMEM((tokens, out_width), full),
             pltpu.VMEM((HALO, channels), half),
             pltpu.VMEM((length + HALO, channels), full),
             pltpu.VMEM((length, channels), full),
@@ -562,16 +660,13 @@
             pltpu.VMEM((16, channels), full),
             pltpu.VMEM((n, 16, channels), full),
             pltpu.VMEM((HALO, channels), half),
-            pltpu.VMEM((capacity, out_width), full),
             pltpu.SemaphoreType.DMA((2,)),
-            *([pair] * 4),
-            *([pltpu.SemaphoreType.DMA((2, n + 1))] * 3),
-            pair,
+            *([pieces] * 8),
             pltpu.SemaphoreType.DMA((2, 1)),
             pair,
         ],
         compiler_params=pltpu.CompilerParams(
-            collective_id=0, has_side_effects=True, vmem_limit_bytes=60 * 1024 * 1024
+            collective_id=0, has_side_effects=True, vmem_limit_bytes=56 * 1024 * 1024
         ),
     )(
         scan.T,
@@ -593,13 +688,13 @@
 
 def fits_fused(tok, routes, up, down):
     n, tp_size = lax.axis_size("ep"), lax.axis_size("tp")
-    if tp_size != 4 or n < 2 or up.shape[0] != 1 or routes.shape[1] != 2:
+    if tp_size != 4 or n != 4 or up.shape[0] != 1 or routes.shape[1] != 2:
         return False
     capacity = slots_per_expert(tok.shape[0], 2, n, tp_size)
-    if capacity % 32 or tok.shape[0] % 32 or up.shape[2] % 128 or down.shape[2] % 256:
+    if capacity % 96 or tok.shape[0] % 32 or up.shape[2] % 128 or down.shape[2] % 256:
         return False
     held = n * capacity * (tok.shape[1] + down.shape[1] + 4 * down.shape[2])
-    return 2 * (held + up.size + down.size + 2 * tok.size) < 40 * 1024 * 1024
+    return 2 * (held + up.size + down.size + 3 * tok.size) < 44 * 1024 * 1024
 
 
 def on_device(

time: 71 us -> 60 us (0.85)
  Pallas kernels: 66.9 us -> 57.8 us
  local copies, waits for them, and re-layouts: 3.2 us -> 1.34 us
    pallas_call x1, Pallas kernels: 66.9 us -> 57.8 us  [fused(): pl.pallas_call(functools.partial(fused_kernel, n, capacity), out_shape=(p...]
    unnamed x2, local copies, waits for them, and re-layouts: 3.2 us -> 1.34 us
where the time goes in v1:
time: 60 us; the launch traced here: 59.8 us
  Pallas kernels  57.8 us (96%)
  local copies, waits for them, and re-layouts  1.34 us (2%)
  between operations  0.64 us (1%)
    pallas_call x1, Pallas kernels, fused(): pl.pallas_call(functools.partial(fused_kernel, n, capacity), out_shape=(p...  57.8 us
    unnamed x2, local copies, waits for them, and re-layouts  1.34 us

profile of v1, /device:TPU:0, one launch (start us, length us, event | category | flops | bytes accessed | tf_op | source)
XLA Modules:
  0.0 59.8 jit_solution(8180492717982690365)
XLA Ops:
  0.6 57.8 %shard_map.140 = (bf16[336,128]{1,0:T(8,128)(2,1)S(1)}, bf16[256,512]{1,0:T(8,128)(2,1)S(1)}) custom-call(bf16[336,128]{1,0:T(8,128)(2,1)} %bitcast.8, bf16[336,128]{1,0:T(8,128)(2,1)} %bitcast.9, bf16[4,336]{1,0:T(4,128)(2,1)} %taps_ref.1, bf16[2,168,168]{2,1,0:T(8,128)(2,1)} %carry_w_ref.1, bf16[2,168,168]{2,1,0:T(8,128)(2,1)} %entry_w_ref.1, ...), custom_call_target="tpu_custom_call" | custom-call | tf_op jit(solution)/shard_map/pallas_call | solution.py:632
  58.5 0.6 %copy.17 = bf16[128,336]{0,1:T(8,128)(2,1)} copy(bf16[128,336]{0,1:T(8,128)(2,1)S(1)} %bitcast.7) | data formatting | bytes 172032
  59.1 0.7 %copy.18 = bf16[256,512]{1,0:T(8,128)(2,1)} copy(bf16[256,512]{1,0:T(8,128)(2,1)S(1)} %get-tuple-element.7) | data formatting | bytes 524288

commit v2 on v1

--- a/solution.py
+++ b/solution.py
@@ -182,12 +182,12 @@
 OWN, NEAR, INNER, OUTER = 0, 1, 2, 3
 PARTS = {OWN: 3, NEAR: 3, INNER: 3, OUTER: 3}
 ORDER = (
-    "D31", "D21", "D32", "P01", "D13", "T31", "P02", "F31", "T21", "D22", "D11", "M31",
-    "T22", "T13", "F13", "F21", "D33", "T11", "D23", "F11", "T32", "D12", "M21", "F22",
-    "T33", "F32", "M32", "G31", "M22", "T23", "S31", "A", "T12", "F12", "F33", "M33",
-    "M11", "G32", "G21", "G01", "M12", "F23", "S32", "M23", "M13", "S21", "G33", "S33",
-    "P03", "G11", "G22", "S11", "S22", "B", "G12", "S12", "G02", "G23", "S23", "G13",
-    "S13", "G03", "S01", "S03", "S02", "C0", "C2", "C3", "C1",
+    "D31", "P01", "D21", "D32", "P02", "D22", "T31", "D12", "D33", "D23", "T32", "F31",
+    "T21", "M31", "T12", "F32", "D13", "T33", "M32", "T22", "A", "G31", "T23", "F33",
+    "G02", "M33", "F21", "D11", "M21", "F23", "F22", "G32", "T13", "M22", "S32", "G33",
+    "S31", "T11", "M23", "G01", "M12", "S33", "M11", "G21", "S02", "S21", "B", "M13",
+    "G23", "G22", "P03", "S01", "S22", "G12", "S23", "S12", "G11", "S11", "G13", "S13",
+    "G03", "C2", "C3", "S03", "C0", "C1",
 )
 
 
@@ -240,6 +240,7 @@
     hm,
     hf,
     rz,
+    out_sems,
     halo_sems,
     carry_sems,
 ):
@@ -252,6 +253,8 @@
     peer = {NEAR: e + 1 - 2 * (e % 2), INNER: 2 - upper, OUTER: 3 - 3 * upper}
     cross_slot = OUTER - (e + upper) % 2
     slot_there = {NEAR: NEAR, INNER: cross_slot, OUTER: cross_slot}
+    tx, tm, tf = (2, INNER, tx), (3, NEAR, tm), (4, INNER, tf)
+    hx, hm, hf = (5, OWN, hx), (6, OWN, hm), (7, OWN, hf)
     tokens, features = tok_ref.shape
     part = features // 4
     width = up.shape[1]
@@ -328,7 +331,6 @@
 
     def begin(copy):
         copy.start()
-        sent.append(copy)
 
     def token_copy(role, c):
         rows = piece(role, c)
@@ -340,8 +342,8 @@
         return pltpu.make_async_remote_copy(
             src_ref=origin,
             dst_ref=toks.at[slot, rows, cols],
-            send_sem=zt.at[0, role, c],
-            recv_sem=zt.at[1, slot, c],
+            send_sem=out_sems.at[0],
+            recv_sem=zt.at[slot - 1, c],
             device_id={"ep": peer[role]},
             device_id_type=MESH,
         )
@@ -353,18 +355,19 @@
         return pltpu.make_async_remote_copy(
             src_ref=view,
             dst_ref=view,
-            send_sem=zt.at[0, slot, c],
-            recv_sem=zt.at[1, slot, c],
+            send_sem=out_sems.at[0],
+            recv_sem=zt.at[slot - 1, c],
             device_id={"ep": peer[slot]},
             device_id_type=MESH,
         )
 
     def shared(view, sems, slot, c, target):
+        kind, first, sems = sems
         return pltpu.make_async_remote_copy(
             src_ref=view,
             dst_ref=view,
-            send_sem=sems.at[0, slot, c],
-            recv_sem=sems.at[1, slot, c],
+            send_sem=out_sems.at[kind],
+            recv_sem=sems.at[slot - first, c],
             device_id={"tp": target},
             device_id_type=MESH,
         )
@@ -382,8 +385,8 @@
         return pltpu.make_async_remote_copy(
             src_ref=res.at[slot, rows],
             dst_ref=back.at[there, rows],
-            send_sem=rz.at[0, slot, c],
-            recv_sem=rz.at[1, there, c],
+            send_sem=out_sems.at[1],
+            recv_sem=rz.at[there - 1, c],
             device_id={"ep": peer[slot]},
             device_id_type=MESH,
         )
@@ -393,8 +396,8 @@
         return pltpu.make_async_remote_copy(
             src_ref=view,
             dst_ref=view,
-            send_sem=rz.at[0, role, c],
-            recv_sem=rz.at[1, role, c],
+            send_sem=out_sems.at[1],
+            recv_sem=rz.at[role - 1, c],
             device_id={"ep": peer[role]},
             device_id_type=MESH,
         )
@@ -537,6 +540,7 @@
         carry_out[8:16, :] = jnp.broadcast_to(state[length - 1 : length, :], (8, channels))
         for j in range(1, n):
             begin(carry_copy(j))
+            sent.append(carry_copy(j))
 
     def scan_finish():
         entering = jnp.zeros((1, channels), jnp.float32)
@@ -607,7 +611,24 @@
             else:
                 tasks[name[0]](int(name[1]), int(name[2]) - 1)
 
+    def sent_all(kind, view):
+        pltpu.make_async_remote_copy(
+            src_ref=view,
+            dst_ref=view,
+            send_sem=out_sems.at[kind],
+            recv_sem=out_sems.at[kind],
+            device_id={"tp": mate},
+            device_id_type=MESH,
+        ).wait_send()
+
     with jax.named_scope("drain"):
+        sent_all(0, toks.at[:, :, f_cols(t)])
+        sent_all(1, res.at[pl.ds(NEAR, n - 1)])
+        sent_all(2, toks.at[pl.ds(INNER, 2), :, f_cols(t)])
+        sent_all(3, toks.at[:, :, f_cols(t)])
+        sent_all(4, toks.at[pl.ds(INNER, 2), :, f_cols(t)])
+        for kind in (5, 6, 7):
+            sent_all(kind, hid.at[:, :, h_cols(t)])
         for copy in sent:
             copy.wait_send()
 
@@ -628,7 +649,8 @@
     vmem = pl.BlockSpec(memory_space=pltpu.VMEM)
     hbm = pl.BlockSpec(memory_space=pl.ANY)
     pair = pltpu.SemaphoreType.DMA((2, n))
-    pieces = pltpu.SemaphoreType.DMA((2, n, max(PARTS.values())))
+    most = max(PARTS.values())
+    two, three, four = (pltpu.SemaphoreType.DMA((k, most)) for k in (2, 3, 4))
     turned, moe = pl.pallas_call(
         functools.partial(fused_kernel, n, capacity),
         out_shape=(
@@ -661,7 +683,13 @@
             pltpu.VMEM((n, 16, channels), full),
             pltpu.VMEM((HALO, channels), half),
             pltpu.SemaphoreType.DMA((2,)),
-            *([pieces] * 8),
+            three,
+            two,
+            three,
+            two,
+            *([four] * 3),
+            three,
+            pltpu.SemaphoreType.DMA((8,)),
             pltpu.SemaphoreType.DMA((2, 1)),
             pair,
         ],

time: 60 us -> 55.3 us (0.922)
  Pallas kernels: 57.8 us -> 53.1 us
    pallas_call x1, Pallas kernels: 57.8 us -> 53.1 us  [fused(): pl.pallas_call(functools.partial(fused_kernel, n, capacity), out_shape=(p...]
where the time goes in v2:
time: 55.3 us; the launch traced here: 55.1 us
  Pallas kernels  53.1 us (96%)
  local copies, waits for them, and re-layouts  1.34 us (2%)
  between operations  0.64 us (1%)
    pallas_call x1, Pallas kernels, fused(): pl.pallas_call(functools.partial(fused_kernel, n, capacity), out_shape=(p...  53.1 us
    unnamed x2, local copies, waits for them, and re-layouts  1.34 us

profile of v2, /device:TPU:0, one launch (start us, length us, event | category | flops | bytes accessed | tf_op | source)
XLA Modules:
  0.0 55.1 jit_solution(15519043708436247140)
XLA Ops:
  0.6 53.1 %shard_map.140 = (bf16[336,128]{1,0:T(8,128)(2,1)S(1)}, bf16[256,512]{1,0:T(8,128)(2,1)S(1)}) custom-call(bf16[336,128]{1,0:T(8,128)(2,1)} %bitcast.8, bf16[336,128]{1,0:T(8,128)(2,1)} %bitcast.9, bf16[4,336]{1,0:T(4,128)(2,1)} %taps_ref.1, bf16[2,168,168]{2,1,0:T(8,128)(2,1)} %carry_w_ref.1, bf16[2,168,168]{2,1,0:T(8,128)(2,1)} %entry_w_ref.1, ...), custom_call_target="tpu_custom_call" | custom-call | tf_op jit(solution)/shard_map/pallas_call | solution.py:654
  53.8 0.6 %copy.17 = bf16[128,336]{0,1:T(8,128)(2,1)} copy(bf16[128,336]{0,1:T(8,128)(2,1)S(1)} %bitcast.7) | data formatting | bytes 172032
  54.4 0.7 %copy.18 = bf16[256,512]{1,0:T(8,128)(2,1)} copy(bf16[256,512]{1,0:T(8,128)(2,1)S(1)} %get-tuple-element.7) | data formatting | bytes 524288

commit v3 on v2

--- a/solution.py
+++ b/solution.py
@@ -182,18 +182,33 @@
 OWN, NEAR, INNER, OUTER = 0, 1, 2, 3
 PARTS = {OWN: 3, NEAR: 3, INNER: 3, OUTER: 3}
 ORDER = (
-    "D31", "P01", "D21", "D32", "P02", "D22", "T31", "D12", "D33", "D23", "T32", "F31",
-    "T21", "M31", "T12", "F32", "D13", "T33", "M32", "T22", "A", "G31", "T23", "F33",
-    "G02", "M33", "F21", "D11", "M21", "F23", "F22", "G32", "T13", "M22", "S32", "G33",
-    "S31", "T11", "M23", "G01", "M12", "S33", "M11", "G21", "S02", "S21", "B", "M13",
-    "G23", "G22", "P03", "S01", "S22", "G12", "S23", "S12", "G11", "S11", "G13", "S13",
-    "G03", "C2", "C3", "S03", "C0", "C1",
+    "D31", "P01", "D21", "D32", "P02", "D22", "H", "T31", "D12", "D33", "D23", "T32",
+    "F31", "T21", "M31", "T12", "F32", "D13", "T33", "M32", "T22", "A", "G31", "T23",
+    "F33", "G02", "M33", "F21", "D11", "M21", "F23", "F22", "G32", "T13", "M22", "S32",
+    "G33", "S31", "T11", "M23", "G01", "M12", "S33", "M11", "G21", "S02", "S21", "B",
+    "M13", "G23", "G22", "P03", "S01", "S22", "G12", "S23", "S12", "G11", "S11", "G13",
+    "S13", "G03", "C2", "C3", "S03", "C0", "C1",
 )
 
 
 def fused_kernel(
     n,
     capacity,
+    scan_hbm,
+    valve_hbm,
+    taps_hbm,
+    carry_w_hbm,
+    entry_w_hbm,
+    lane_hbm,
+    jump_hbm,
+    tok_hbm,
+    gain_hbm,
+    route_hbm,
+    score_hbm,
+    up_hbm,
+    down_hbm,
+    scan_out,
+    moe_out,
     scan_ref,
     valve_ref,
     taps_ref,
@@ -205,10 +220,6 @@
     gain_ref,
     route_ref,
     score_ref,
-    up_hbm,
-    down_hbm,
-    scan_out,
-    moe_out,
     up,
     down,
     normed,
@@ -278,31 +289,49 @@
         pl.semaphore_signal(barrier, inc=1, device_id={"ep": (e + j) % n}, device_id_type=MESH)
     for other in (mate, across):
         pl.semaphore_signal(barrier, inc=1, device_id={"tp": other}, device_id_type=MESH)
-    load_up = pltpu.make_async_copy(up_hbm.at[0], up, load_sems.at[0])
-    load_down = pltpu.make_async_copy(down_hbm.at[0], down, load_sems.at[1])
-    load_up.start()
-    load_down.start()
+    rows_step = tokens // 4
+
+    def token_load(i):
+        rows = pl.ds(pl.multiple_of(i * rows_step, rows_step), rows_step)
+        return pltpu.make_async_copy(tok_hbm.at[rows], tok_ref.at[rows], load_sems.at[i])
+
+    sources = (
+        (gain_hbm, gain_ref),
+        (route_hbm, route_ref),
+        (up_hbm.at[0], up),
+        (scan_hbm, scan_ref),
+        (taps_hbm, taps_ref),
+        (lane_hbm, lane_ref),
+        (jump_hbm, jump_ref),
+        (carry_w_hbm, carry_w_ref),
+        (entry_w_hbm, entry_w_ref),
+        (score_hbm, score_ref),
+        (valve_hbm, valve_ref),
+        (down_hbm.at[0], down),
+    )
+    loads = [
+        pltpu.make_async_copy(origin, place, load_sems.at[4 + i])
+        for i, (origin, place) in enumerate(sources)
+    ]
+    for i in range(4):
+        token_load(i).start()
+    for load in loads:
+        load.start()
+    load_gain, load_route, load_up = loads[:3]
+    load_scan, load_late, load_down = loads[3], loads[4:11], loads[11]
     channels, length = scan_ref.shape
-
-    with jax.named_scope("halo_prep"):
-        turned = scan_ref[...].astype(jnp.float32).T
-        padded[HALO:, :] = turned
-        halo_out[...] = turned[length - HALO :, :].astype(jnp.bfloat16)
-
-    rows_step = 64
 
     def norm_rows(i, _):
         rows = pl.ds(pl.multiple_of(i * rows_step, rows_step), rows_step)
+        token_load(i).wait()
         x = tok_ref[rows, :].astype(jnp.float32)
         centered = x - jnp.sum(x, axis=1, keepdims=True) * (1.0 / features)
         var = jnp.sum(centered * centered, axis=1, keepdims=True) * (1.0 / features)
         normed[rows, :] = (centered * lax.rsqrt(var + 1e-05) * gain_ref[...]).astype(jnp.bfloat16)
         return 0
 
-    with jax.named_scope("norm"):
-        lax.fori_loop(0, tokens // rows_step, norm_rows, 0)
-
     with jax.named_scope("rank"):
+        load_route.wait()
         routes = route_ref[...].astype(jnp.float32)
         first, second = routes[0:1, :], routes[1:2, :]
         erow = lax.broadcasted_iota(jnp.int32, (rank_rows.shape[0], tokens), 0).astype(jnp.float32)
@@ -316,6 +345,10 @@
         )
         rank_rows[...] = jnp.where(hit, rank, -1.0)
 
+    with jax.named_scope("norm"):
+        load_gain.wait()
+        lax.fori_loop(0, tokens // rows_step, norm_rows, 0)
+
     def picker(expert, start, size):
         slots = start + lax.broadcasted_iota(jnp.int32, (size, tokens), 0)
         hits = slots.astype(jnp.float32) == rank_rows[pl.ds(expert, 1), :]
@@ -325,7 +358,6 @@
         pl.semaphore_wait(barrier, n + 1)
 
     send_halo = remote(halo_out, halo, halo_sems, 0, ep=(e + 1) % n)
-    send_halo.start()
     sent = [send_halo]
     waited = []
 
@@ -511,7 +543,16 @@
     def carry_copy(j):
         return remote(carry_out, carry_in.at[j], carry_sems, j, ep=(e + n - j) % n)
 
+    def halo_out_now():
+        load_scan.wait()
+        turned = scan_ref[...].astype(jnp.float32).T
+        padded[HALO:, :] = turned
+        halo_out[...] = turned[length - HALO :, :].astype(jnp.bfloat16)
+        send_halo.start()
+
     def scan_local():
+        for load in load_late:
+            load.wait()
         send_halo.wait_recv()
         padded[0:HALO, :] = jnp.where(e > 0, halo[...].astype(jnp.float32), 0.0)
         taps = taps_ref[...].astype(jnp.float32)
@@ -603,6 +644,8 @@
         with jax.named_scope(name):
             if name == "A":
                 scan_local()
+            elif name == "H":
+                halo_out_now()
             elif name == "B":
                 scan_finish()
                 plan_combine()
@@ -635,6 +678,17 @@
 
 def slots_per_expert(tokens, top_count, experts, tp_size):
     return tp_size * ((3 * tokens * top_count + 2 * experts * tp_size - 1) // (2 * experts * tp_size))
+
+
+def write_out(turned_ref, moe_ref, turned_out, moe_out, sems):
+    copies = (
+        pltpu.make_async_copy(turned_ref, turned_out, sems.at[0]),
+        pltpu.make_async_copy(moe_ref, moe_out, sems.at[1]),
+    )
+    for copy in copies:
+        copy.start()
+    for copy in copies:
+        copy.wait()
 
 
 def fused(*arrays):
@@ -651,15 +705,29 @@
     pair = pltpu.SemaphoreType.DMA((2, n))
     most = max(PARTS.values())
     two, three, four = (pltpu.SemaphoreType.DMA((k, most)) for k in (2, 3, 4))
+    small = (
+        scan.T,
+        valve.T,
+        taps,
+        carry_w,
+        entry_w,
+        lane,
+        jump.reshape(1, -1),
+        tok,
+        gain.reshape(1, -1),
+        routes.T,
+        scores.T,
+    )
     turned, moe = pl.pallas_call(
         functools.partial(fused_kernel, n, capacity),
         out_shape=(
             pltpu.VMEM((channels, length), half),
             pltpu.VMEM((tokens, out_width), half),
         ),
-        in_specs=[vmem] * 11 + [hbm] * 2,
+        in_specs=[hbm] * 13,
         out_specs=(vmem, vmem),
         scratch_shapes=[
+            *(pltpu.VMEM(a.shape, a.dtype) for a in small),
             pltpu.VMEM((features, width), half),
             pltpu.VMEM((units, out_width), half),
             pltpu.VMEM((tokens, features), half),
@@ -682,7 +750,7 @@
             pltpu.VMEM((16, channels), full),
             pltpu.VMEM((n, 16, channels), full),
             pltpu.VMEM((HALO, channels), half),
-            pltpu.SemaphoreType.DMA((2,)),
+            pltpu.SemaphoreType.DMA((16,)),
             three,
             two,
             three,
@@ -696,21 +764,18 @@
         compiler_params=pltpu.CompilerParams(
             collective_id=0, has_side_effects=True, vmem_limit_bytes=56 * 1024 * 1024
         ),
-    )(
-        scan.T,
-        valve.T,
-        taps,
-        carry_w,
-        entry_w,
-        lane,
-        jump.reshape(1, -1),
-        tok,
-        gain.reshape(1, -1),
-        routes.T,
-        scores.T,
-        up,
-        down,
-    )
+    )(*small, up, down)
+    turned, moe = pl.pallas_call(
+        write_out,
+        out_shape=(
+            jax.ShapeDtypeStruct((channels, length), half),
+            jax.ShapeDtypeStruct((tokens, out_width), half),
+        ),
+        in_specs=[hbm] * 2,
+        out_specs=(hbm, hbm),
+        scratch_shapes=[pltpu.SemaphoreType.DMA((2,))],
+        compiler_params=pltpu.CompilerParams(vmem_limit_bytes=2 * 1024 * 1024),
+    )(turned, moe)
     return turned.T, moe
 
 

time: 55.3 us -> 54.6 us (0.987)
  local copies, waits for them, and re-layouts: 1.34 us -> 0 us
  Pallas kernels: 53.1 us -> 53.7 us
    unnamed x2 -> x0, local copies, waits for them, and re-layouts: 1.34 us -> none
    pallas_call x0 -> x1, Pallas kernels: none -> 0.75 us  [fused(): pl.pallas_call(write_out, out_shape=(jax.ShapeDtypeStruct((channels, leng...]
where the time goes in v3:
time: 54.6 us; the launch traced here: 54.5 us
  Pallas kernels  53.7 us (98%)
  between operations  0.8 us (1%)
    pallas_call x1, Pallas kernels, fused(): pl.pallas_call(functools.partial(fused_kernel, n, capacity), out_shape=(p...  52.9 us

profile of v3, /device:TPU:0, one launch (start us, length us, event | category | flops | bytes accessed | tf_op | source)
XLA Modules:
  0.0 54.5 jit_solution(12532863491397785496)
XLA Ops:
  0.6 52.9 %shard_map.140 = (bf16[336,128]{1,0:T(8,128)(2,1)S(1)}, bf16[256,512]{1,0:T(8,128)(2,1)S(1)}) custom-call(bf16[336,128]{1,0:T(8,128)(2,1)} %bitcast.7, bf16[336,128]{1,0:T(8,128)(2,1)} %bitcast.8, bf16[4,336]{1,0:T(4,128)(2,1)} %taps_hbm.1, bf16[2,168,168]{2,1,0:T(8,128)(2,1)} %carry_w_hbm.1, bf16[2,168,168]{2,1,0:T(8,128)(2,1)} %entry_w_hbm.1, ...), custom_call_target="tpu_custom_call" | custom-call | tf_op jit(solution)/shard_map/pallas_call | solution.py:721
  53.6 0.8 %shard_map.141 = (bf16[336,128]{1,0:T(8,128)(2,1)}, bf16[256,512]{1,0:T(8,128)(2,1)}) custom-call(bf16[336,128]{1,0:T(8,128)(2,1)S(1)} %get-tuple-element.6.turned_ref, bf16[256,512]{1,0:T(8,128)(2,1)S(1)} %get-tuple-element.7.moe_ref), custom_call_target="tpu_custom_call" | custom-call | tf_op jit(solution)/shard_map/pallas_call | solution.py:768
